TPU v7x, 128 devices: a whole 4x4x4 slice. The times are simulated.
128 devices in a mesh: sp: 16 (over z, y), fs: 4 (over x), tp: 2 (over core).
Axes of the slice: x: 4, y: 4, z: 4, core: 2. Of those that a mesh axis runs over, the one named last changes fastest.
Arguments:
- tokens: bfloat16 [65536, 2048], P(('fs', 'sp', 'tp')), parts along dimension 0, may hold values from -6 to 6
- norm_gain: float32 [2048], replicated, may hold values from 0.1 to 1.9
- w_pool: bfloat16 [2048, 1024], P(None, 'tp'), may hold values from -0.125 to 0.125
- w_query: bfloat16 [2048, 1024], P(None, 'tp'), may hold values from -0.125 to 0.125
- w_key: bfloat16 [2048, 1024], P(None, 'tp'), may hold values from -0.125 to 0.125
- w_value: bfloat16 [2048, 1024], P(None, 'tp'), may hold values from -0.125 to 0.125
- w_gate: bfloat16 [2048, 1024], P(None, 'tp'), may hold values from -0.125 to 0.125
- pool_mix: bfloat16 [4, 256, 256], P('tp'), may hold values from -0.375 to 0.375
- pool_bias: float32 [4, 256], P('tp'), may hold values from -3 to 3
- pool_gain: float32 [1024], P('tp'), may hold values from 0.1 to 1.9
- ret_gain: float32 [1024], P('tp'), may hold values from 0.1 to 1.9
- w_out_pool: bfloat16 [1024, 2048], P('tp'), may hold values from -0.125 to 0.125
- w_out_ret: bfloat16 [1024, 2048], P('tp'), may hold values from -0.125 to 0.125
Outputs:
- mixed: bfloat16 [65536, 2048], P(('fs', 'sp', 'tp')), parts along dimension 0
There are 4 independent parts, one for each index of `fs`. A program takes and returns all parts, laid end to end along the dimension named above; an argument that names none is the same for every part. Nothing has to cross between parts.
All inputs are finite; a program needn't handle non-finite values.
Results may differ from a plain program's by a relative error of at most 0.012.
Values may be sent and summed in bfloat16 or wider, within the bound.
No kernel may reach another device: no remote copies, remote signals or barrier semaphores. Data moves between devices by JAX's collectives and lax.ppermute only.
A program may use at most 128 MiB of HBM per device.

v0:
```python
import jax
import jax.numpy as jnp
from jax import lax
from jax.sharding import Mesh
from jax.sharding import PartitionSpec as P

GROUP_DIM = 256
HEAD_DIM = 128
BLOCK = 128
SP = ("sp_0", "sp_1")
FS_SP_TP = ("fs", "sp_0", "sp_1", "tp")


rim_len = 16


def joined_along(parts, dim):
    parts = jnp.moveaxis(parts, 0, dim)
    lengths = parts.shape
    return parts.reshape(*lengths[:dim], lengths[dim] * lengths[dim + 1], *lengths[dim + 2 :])


def work_in_pieces(array, axis, dim, work, out_dim):
    span = array.shape[dim]
    pieces = jnp.split(array, 2, axis=dim) if span % 2 == 0 else [array]
    leading = jnp.arange(lax.axis_size(axis)) * span
    parts = [lax.all_gather(slab, axis) for slab in pieces]
    made = [jax.vmap(work)(b, leading + k * (span // len(pieces))) for k, b in enumerate(parts)]
    return joined_along(jnp.concatenate(made, axis=out_dim + 1), out_dim)


def nothing_yet(array, identity):
    return jax.tree.map(
        lambda a, e: jnp.broadcast_to(jnp.asarray(e, a.dtype), a.shape), array, identity
    )


def carried_in(array, axes, combine, identity):
    before = start = nothing_yet(array, identity)
    running = array
    for axis in reversed(axes):
        length, position = (lax.axis_size(axis), lax.axis_index(axis))
        pieces = jax.tree.map(
            lambda part, kind: lax.all_gather(part.astype(kind), axis),
            running,
            (jnp.bfloat16, jnp.bfloat16),
        )
        inside, running = (start, start)
        for k in range(length):
            passed = k < position
            running = combine(
                running, jax.tree.map(lambda part, own: part[k].astype(own.dtype), pieces, array)
            )
            inside = jax.tree.map(lambda new, old: jnp.where(passed, new, old), running, inside)
        before = combine(inside, before)
    return before


def shifted(array, axis, by):
    length = lax.axis_size(axis)
    pairs = [(i, i + by) for i in range(length) if 0 <= i + by < length]
    return lax.ppermute(array, axis, pairs)


def split_up(array, dim, length):
    before, after = (array.shape[:dim], array.shape[dim + 1 :])
    return jnp.moveaxis(array.reshape(*before, length, -1, *after), dim, 0)


def sent_and_summed(array, axis, dim):
    length = lax.axis_size(axis)
    parts = lax.all_to_all(split_up(array, dim, length), axis, 0, 0, tiled=True)
    return jnp.sum(parts.astype(jnp.float32), axis=0)


def rotary(values, positions):
    half = values.shape[-1] // 2
    inverse = 10000.0 ** (-jnp.arange(half, dtype=jnp.float32) / half)
    angles = positions[:, None] * inverse[None, :]
    cosine = jnp.cos(angles)[:, None, :]
    sine = jnp.sin(angles)[:, None, :]
    first = values[..., :half]
    second = values[..., half:]
    return jnp.concatenate(
        [first * cosine - second * sine, second * cosine + first * sine], axis=-1
    )


def retain(query, key, value, log_decay):
    length, heads_here = (query.shape[0], query.shape[1])
    blocks = length // BLOCK

    def split(values):
        return values.reshape(blocks, BLOCK, heads_here, HEAD_DIM).transpose(0, 2, 1, 3)

    steps = jnp.arange(BLOCK, dtype=jnp.float32)
    apart = steps[:, None] - steps[None, :]
    inner = jnp.where(
        apart[None] >= 0, jnp.exp(log_decay[:, None, None] * jnp.maximum(apart, 0.0)[None]), 0.0
    )
    query_decay = jnp.exp(log_decay[:, None] * (steps[None, :] + 1.0))
    key_decay = jnp.exp(log_decay[:, None] * (BLOCK - 1.0 - steps[None, :]))
    block_decay = jnp.exp(log_decay * BLOCK)

    def advance(state, pieces):
        qb, kb, vb = pieces
        scores = jnp.einsum("hid,hjd->hij", qb, kb) * inner
        out = jnp.einsum("hij,hje->hie", scores, vb)
        out = out + jnp.einsum("hid,hde->hie", qb, state) * query_decay[:, :, None]
        state = state * block_decay[:, None, None] + jnp.einsum(
            "hjd,hje->hde", kb * key_decay[:, :, None], vb
        )
        return (state, out)

    start = jnp.zeros((heads_here, HEAD_DIM, HEAD_DIM), jnp.float32)
    state, outs = lax.scan(advance, start, (split(query), split(key), split(value)))
    return (outs.transpose(0, 2, 1, 3).reshape(length, heads_here, HEAD_DIM), state)


def per_device(
    tokens,
    norm_gain,
    w_pool,
    w_query,
    w_key,
    w_value,
    w_gate,
    pool_mix,
    pool_bias,
    pool_gain,
    ret_gain,
    w_out_pool,
    w_out_ret,
):
    tp_index = lax.axis_index("tp")
    sp_index = lax.axis_index(SP)
    xf = tokens.astype(jnp.float32)
    normed = (xf * lax.rsqrt(jnp.mean(xf * xf, axis=-1, keepdims=True) + 1e-06) * norm_gain).astype(
        jnp.bfloat16
    )
    weights = (w_pool, w_query, w_key, w_value, w_gate)

    def project(piece, start):
        return jnp.concatenate(
            [
                jnp.dot(piece, weight, preferred_element_type=jnp.float32).astype(jnp.bfloat16)
                for weight in weights
            ],
            axis=1,
        )

    projected = work_in_pieces(normed, "tp", 0, project, 0)
    width_pool = w_pool.shape[1]
    width_ret = w_query.shape[1]
    pool_in = projected[:, :width_pool]
    query = projected[:, width_pool : width_pool + width_ret]
    key = projected[:, width_pool + width_ret : width_pool + 2 * width_ret]
    value = projected[:, width_pool + 2 * width_ret : width_pool + 3 * width_ret]
    gate = projected[:, width_pool + 3 * width_ret :]
    length = projected.shape[0]
    seq_len = length * lax.axis_size(SP)
    positions = (sp_index * length + jnp.arange(length, dtype=jnp.int32)).astype(jnp.float32)
    heads_here = width_ret // HEAD_DIM
    total_heads = heads_here * lax.axis_size("tp")
    head_ids = (tp_index * heads_here + jnp.arange(heads_here, dtype=jnp.int32)).astype(jnp.float32)
    log_decay = -(2.0 ** (-5)) * (seq_len / 16.0) ** (-2.0 * head_ids / (total_heads - 1))
    qf = rotary(query.astype(jnp.float32).reshape(length, heads_here, HEAD_DIM), positions)
    kf = rotary(
        key.astype(jnp.float32).reshape(length, heads_here, HEAD_DIM), positions
    ) * HEAD_DIM ** (-0.5)
    vf = value.astype(jnp.float32).reshape(length, heads_here, HEAD_DIM)
    local_out, local_state = retain(qf, kf, vf, log_decay)
    device_decay = jnp.exp(log_decay * length)
    empty_state = jnp.zeros_like(local_state)

    def combine(earlier, later):
        return (earlier[0] * later[0], later[1] + later[0][:, None, None] * earlier[1])

    scanned = carried_in(
        (device_decay, local_state), SP, combine, (jnp.ones_like(device_decay), empty_state)
    )
    incoming = scanned[1]
    rim = shifted(pool_in[length - rim_len :], SP, 1)
    padded = jnp.concatenate([rim, pool_in], axis=0).astype(jnp.float32)
    groups_here = width_pool // GROUP_DIM
    group_local = jnp.arange(width_pool, dtype=jnp.int32) // GROUP_DIM
    window = jnp.power(2, 1 + tp_index * groups_here + group_local)
    window_sum = jnp.zeros((length, width_pool), jnp.float32)
    for offset in range(rim_len):
        window_sum = window_sum + jnp.where(
            offset < window[None, :], padded[rim_len - offset : rim_len - offset + length], 0.0
        )
    count = jnp.minimum(positions[:, None] + 1.0, window[None, :].astype(jnp.float32))
    diff = (
        (window_sum / count - padded[rim_len:])
        .astype(jnp.bfloat16)
        .reshape(length, groups_here, GROUP_DIM)
    )
    mixed_groups = (
        jnp.einsum("lgc,gcd->lgd", diff, pool_mix, preferred_element_type=jnp.float32)
        + pool_bias[None]
    )
    pool_out = (mixed_groups.reshape(length, width_pool) * pool_gain[None, :]).astype(jnp.bfloat16)
    local_steps = jnp.arange(length, dtype=jnp.float32)
    carry_decay = jnp.exp(log_decay[None, :] * (local_steps[:, None] + 1.0))
    raw = local_out + jnp.einsum("lhd,hde->lhe", qf * carry_decay[:, :, None], incoming)
    mean = jnp.mean(raw, axis=-1, keepdims=True)
    var = jnp.mean(jnp.square(raw - mean), axis=-1, keepdims=True)
    normalized = ((raw - mean) * lax.rsqrt(var + 1e-06)).reshape(length, width_ret) * ret_gain[
        None, :
    ]
    ret_out = (jax.nn.silu(gate.astype(jnp.float32)) * normalized).astype(jnp.bfloat16)
    summed = jnp.dot(pool_out, w_out_pool, preferred_element_type=jnp.float32) + jnp.dot(
        ret_out, w_out_ret, preferred_element_type=jnp.float32
    )
    rounded = lax.optimization_barrier(summed.astype(jnp.bfloat16))
    mixed = sent_and_summed(rounded.astype(jnp.float32).astype(jnp.bfloat16), "tp", 0)
    return mixed.astype(jnp.bfloat16)


def solution(mesh):
    finer = Mesh(
        mesh.devices.reshape(4, 4, mesh.shape["fs"], mesh.shape["tp"]), ("sp_0", "sp_1", "fs", "tp")
    )
    placed = (
        P(FS_SP_TP, None),
        P(),
        P(None, "tp"),
        P(None, "tp"),
        P(None, "tp"),
        P(None, "tp"),
        P(None, "tp"),
        P("tp", None, None),
        P("tp", None),
        P("tp"),
        P("tp"),
        P("tp", None),
        P("tp", None),
    )
    return jax.shard_map(
        per_device, mesh=finer, in_specs=placed, out_specs=P(FS_SP_TP, None), check_vma=False
    )
```

profile of v0, /device:TPU:1, one launch (start us, length us, event | category | flops | bytes accessed | tf_op | source)
XLA Modules:
  0.0 200.5 jit_solution(12313396916690896651)
XLA Ops:
  17.4 8.8 %all-gather.3 = bf16[4,1,4]{2,1,0:T(2,128)(2,1)S(1)} all-gather(bf16[1,1,4]{2,1,0:T(2,128)(2,1)S(1)} %convert_bitcast_fusion.5), channel_id=1, replica_groups=mesh['sp_0'=4,'sp_1'=4,'fs'=4,'tp'=2] {'sp_1'}, dimensions={0}, use_global_device_ids=true | all-gather | bytes 40 | tf_op jit(solution)/shard_map/all_gather | solution.py:44
  26.2 9.0 %all-gather.4 = bf16[4,1,4]{2,1,0:T(2,128)(2,1)S(1)} all-gather(bf16[1,1,4]{2,1,0:T(2,128)(2,1)S(1)} %fusion.217), channel_id=1, replica_groups=mesh['sp_0'=4,'sp_1'=4,'fs'=4,'tp'=2] {'sp_0'}, dimensions={0}, use_global_device_ids=true | all-gather | bytes 40 | tf_op jit(solution)/shard_map/all_gather | solution.py:44
  38.8 3.7 %fusion.95 = bf16[2,256,2560]{2,1,0:T(8,128)(2,1)} fusion(bf16[2,256,2048]{2,1,0:T(8,128)(2,1)} %bitcast.295, bf16[2048,512]{1,0:T(8,128)(2,1)S(1)} %copy-done), kind=kOutput, calls=%fused_computation.118 | convolution fusion | flops 1074003968 | bytes 4718592 | tf_op jit(solution)/shard_map/vmap()/dot_general | solution.py:146
  42.6 2.6 %all-gather.8.cloned.1.call-done = bf16[512,2048]{1,0:T(8,128)(2,1)} async-done(((bf16[256,2048]{1,0:T(8,128)(2,1)}), bf16[512,2048]{1,0:T(8,128)(2,1)}) %all-gather.8.cloned.1.call-update) | async-done | bytes 2097168 | tf_op jit(solution)/shard_map/all_gather | solution.py:27
  45.1 3.0 %fusion.89 = bf16[2,256,2560]{2,1,0:T(8,128)(2,1)S(1)} fusion(bf16[2,256,2048]{2,1,0:T(8,128)(2,1)} %bitcast.300, bf16[2048,512]{1,0:T(8,128)(2,1)S(1)} %copy-done), kind=kOutput, calls=%fused_computation.116 | convolution fusion | flops 1074003968 | bytes 4718592 | tf_op jit(solution)/shard_map/vmap()/dot_general | solution.py:146
  65.3 3.9 %collective-permute-start = (bf16[16,512]{0,1:T(8,128)(2,1)}, bf16[16,512]{0,1:T(8,128)(2,1)}, u32[]{:S(2)}, u32[]{:S(2)}) collective-permute-start(bf16[16,512]{0,1:T(8,128)(2,1)} %copy.57), channel_id=1, source_target_pairs={{0,8},{8,16},{16,24},{24,32},{32,40},{40,48},{48,56},{56,64},{64,7... | collective-permute-start | bytes 49160 | tf_op jit(solution)/shard_map/ppermute | solution.py:62
  82.6 2.8 %fusion.58 = f32[8,4,128,128]{2,0,3,1:T(8,128)} fusion(f32[8,128,4,64]{1,0,3,2:T(8,128)S(1)} %bitcast.291, f32[8,128,4,64]{1,0,3,2:T(8,128)} %bitcast.292), kind=kLoop, calls=%fused_computation.82 | loop fusion | flops 1048576 | bytes 4194304 | tf_op jit(solution)/shard_map/transpose | solution.py:94
  85.5 35.5 %while.15 = (s32[]{:T(128)}, f32[4,128,128]{2,1,0:T(8,128)S(1)}, f32[8,4,128,128]{3,2,1,0:T(8,128)}, f32[8,4,128,128]{2,0,3,1:T(8,128)}, f32[8,4,128,128]{2,0,3,...) while((s32[]{:T(128)}, f32[4,128,128]{2,1,0:T(8,128)S(1)}, ...), condition=%wide.region_2.3_spmd.clone.clone.clone, body=%wide.region_1.2_spmd.clone.clone.clone.sunk | while | flops 67830800 | bytes 4549843 | solution.py:116
  85.5 2.6 %constant_dynamic-slice_fusion.3 = (f32[1,4,128,128]{2,0,3,1:T(1,128)S(1)}, f32[1,4,128,128]{2,0,3,1:T(1,128)S(1)}) fusion(f32[8,4,128,128]{2,0,3,1:T(8,128)} %get-tuple-element.388, s32[]{:T(128)S(6)} %copy.79, f32[8,4,128,128]{2,0,3,1:T(8,128)} %get-tuple-element.387), kind=kLoop, calls=%fused_computation.31.clone.1 | loop fusion | bytes 1048580 | tf_op jit(solution)/shard_map/while/body/jit(dynamic_index_in_dim)/dynamic_slice | solution.py:116
  90.0 2.6 %constant_dynamic-slice_fusion.3 = (f32[1,4,128,128]{2,0,3,1:T(1,128)S(1)}, f32[1,4,128,128]{2,0,3,1:T(1,128)S(1)}) fusion(f32[8,4,128,128]{2,0,3,1:T(8,128)} %get-tuple-element.388, s32[]{:T(128)S(6)} %copy.79, f32[8,4,128,128]{2,0,3,1:T(8,128)} %get-tuple-element.387), kind=kLoop, calls=%fused_computation.31.clone.1 | loop fusion | bytes 1048580 | tf_op jit(solution)/shard_map/while/body/jit(dynamic_index_in_dim)/dynamic_slice | solution.py:116
  94.4 2.6 %constant_dynamic-slice_fusion.3 = (f32[1,4,128,128]{2,0,3,1:T(1,128)S(1)}, f32[1,4,128,128]{2,0,3,1:T(1,128)S(1)}) fusion(f32[8,4,128,128]{2,0,3,1:T(8,128)} %get-tuple-element.388, s32[]{:T(128)S(6)} %copy.79, f32[8,4,128,128]{2,0,3,1:T(8,128)} %get-tuple-element.387), kind=kLoop, calls=%fused_computation.31.clone.1 | loop fusion | bytes 1048580 | tf_op jit(solution)/shard_map/while/body/jit(dynamic_index_in_dim)/dynamic_slice | solution.py:116
  98.9 2.6 %constant_dynamic-slice_fusion.3 = (f32[1,4,128,128]{2,0,3,1:T(1,128)S(1)}, f32[1,4,128,128]{2,0,3,1:T(1,128)S(1)}) fusion(f32[8,4,128,128]{2,0,3,1:T(8,128)} %get-tuple-element.388, s32[]{:T(128)S(6)} %copy.79, f32[8,4,128,128]{2,0,3,1:T(8,128)} %get-tuple-element.387), kind=kLoop, calls=%fused_computation.31.clone.1 | loop fusion | bytes 1048580 | tf_op jit(solution)/shard_map/while/body/jit(dynamic_index_in_dim)/dynamic_slice | solution.py:116
  103.3 2.6 %constant_dynamic-slice_fusion.3 = (f32[1,4,128,128]{2,0,3,1:T(1,128)S(1)}, f32[1,4,128,128]{2,0,3,1:T(1,128)S(1)}) fusion(f32[8,4,128,128]{2,0,3,1:T(8,128)} %get-tuple-element.388, s32[]{:T(128)S(6)} %copy.79, f32[8,4,128,128]{2,0,3,1:T(8,128)} %get-tuple-element.387), kind=kLoop, calls=%fused_computation.31.clone.1 | loop fusion | bytes 1048580 | tf_op jit(solution)/shard_map/while/body/jit(dynamic_index_in_dim)/dynamic_slice | solution.py:116
  107.8 2.6 %constant_dynamic-slice_fusion.3 = (f32[1,4,128,128]{2,0,3,1:T(1,128)S(1)}, f32[1,4,128,128]{2,0,3,1:T(1,128)S(1)}) fusion(f32[8,4,128,128]{2,0,3,1:T(8,128)} %get-tuple-element.388, s32[]{:T(128)S(6)} %copy.79, f32[8,4,128,128]{2,0,3,1:T(8,128)} %get-tuple-element.387), kind=kLoop, calls=%fused_computation.31.clone.1 | loop fusion | bytes 1048580 | tf_op jit(solution)/shard_map/while/body/jit(dynamic_index_in_dim)/dynamic_slice | solution.py:116
  112.2 2.6 %constant_dynamic-slice_fusion.3 = (f32[1,4,128,128]{2,0,3,1:T(1,128)S(1)}, f32[1,4,128,128]{2,0,3,1:T(1,128)S(1)}) fusion(f32[8,4,128,128]{2,0,3,1:T(8,128)} %get-tuple-element.388, s32[]{:T(128)S(6)} %copy.79, f32[8,4,128,128]{2,0,3,1:T(8,128)} %get-tuple-element.387), kind=kLoop, calls=%fused_computation.31.clone.1 | loop fusion | bytes 1048580 | tf_op jit(solution)/shard_map/while/body/jit(dynamic_index_in_dim)/dynamic_slice | solution.py:116
  116.6 2.6 %constant_dynamic-slice_fusion.3 = (f32[1,4,128,128]{2,0,3,1:T(1,128)S(1)}, f32[1,4,128,128]{2,0,3,1:T(1,128)S(1)}) fusion(f32[8,4,128,128]{2,0,3,1:T(8,128)} %get-tuple-element.388, s32[]{:T(128)S(6)} %copy.79, f32[8,4,128,128]{2,0,3,1:T(8,128)} %get-tuple-element.387), kind=kLoop, calls=%fused_computation.31.clone.1 | loop fusion | bytes 1048580 | tf_op jit(solution)/shard_map/while/body/jit(dynamic_index_in_dim)/dynamic_slice | solution.py:116
  121.0 2.9 %copy.45 = f32[8,128,4,128]{1,0,3,2:T(8,128)} copy(f32[8,128,4,128]{3,1,2,0:T(8,128)} %bitcast.294) | data formatting | bytes 4194304 | tf_op jit(solution)/shard_map/transpose | solution.py:117
  123.9 2.7 %reshape.443 = f32[1024,4,128]{0,2,1:T(8,128)} reshape(f32[8,128,4,128]{1,0,3,2:T(8,128)} %copy.45) | data formatting | bytes 4194304 | tf_op jit(solution)/shard_map/reshape | solution.py:117
  126.7 11.0 %all-gather.2 = bf16[16,128,128]{2,1,0:T(8,128)(2,1)S(1)} all-gather(bf16[4,128,128]{2,1,0:T(8,128)(2,1)S(1)} %convert_element_type.304), channel_id=4, replica_groups=mesh['sp_0'=4,'sp_1'=4,'fs'=4,'tp'=2] {'sp_1'}, dimensions={0}, use_global_device_ids=true | all-gather | bytes 655360 | tf_op jit(solution)/shard_map/all_gather | solution.py:44
  137.8 10.0 %all_gather.37 = bf16[4,4,128,128]{3,2,1,0:T(8,128)(2,1)S(1)} all-gather(bf16[1,4,128,128]{3,2,1,0:T(8,128)(2,1)S(1)} %fusion.159), channel_id=1, replica_groups=mesh['sp_0'=4,'sp_1'=4,'fs'=4,'tp'=2] {'sp_0'}, dimensions={0}, use_global_device_ids=true | all-gather | bytes 655360 | tf_op jit(solution)/shard_map/all_gather | solution.py:44
  155.1 11.4 %fusion.83 = bf16[1024,512]{0,1:T(8,128)(2,1)S(1)} fusion(f32[1040,512]{0,1:T(8,128)S(1)} %maximum_convert_fusion, f32[512]{0:T(512)S(1)} %fusion.210, f32[1024]{0:T(1024)S(1)} %broadcast_add_fusion, pred[512]{0:T(512)(128)(4,1)S(1)} %copy-done.34, pred[512]{0:T(512)(128)(4,1)S(1)} %copy-done.35, pred[512]{0:T(512)(128)(4,1)S(1)} %copy-done.30, ...), kind=kLoop, calls=%fused_computation.112 | loop fusion | flops 18350080 | bytes 34617344 | tf_op jit(solution)/shard_map/convert_element_type | solution.py:196
  171.3 3.9 %add_convert_fusion = bf16[1024,2048]{1,0:T(8,128)(2,1)S(1)} fusion(f32[1024,2048]{1,0:T(8,128)S(1)} %fusion.226, bf16[512,2048]{1,0:T(8,128)(2,1)S(1)} %copy-done.43, f32[1024,512]{1,0:T(8,128)S(1)} %copy-done.11, bf16[1024,2560]{1,0:T(8,128)(2,1)} %bitcast.282, f32[512]{0:T(512)S(1)} %copy-done.46), kind=kOutput, calls=%fused_computation.36 | convolution fusion | flops 2155872256 | bytes 17827840 | tf_op jit(solution)/shard_map/dot_general | solution.py:213
  175.2 13.4 %all_to_all.5 = bf16[2,512,2048]{2,1,0:T(8,128)(2,1)} all-to-all(bf16[2,512,2048]{2,1,0:T(8,128)(2,1)S(1)} %bitcast.290), channel_id=1, replica_groups=mesh['sp_0'=4,'sp_1'=4,'fs'=4,'tp'=2] {'tp'}, dimensions={0} | all-to-all | bytes 8388608 | tf_op jit(solution)/shard_map/all_to_all | solution.py:72
  188.5 5.1 %reduce_sum.42 = bf16[512,2048]{1,0:T(8,128)(2,1)} reduce(bf16[2,512,2048]{2,1,0:T(8,128)(2,1)} %all_to_all.5, bf16[]{:T(256)} %constant.178.clone.1), dimensions={0}, to_apply=%region_5.6 | reduce | flops 1048576 | bytes 6291458 | tf_op jit(solution)/shard_map/reduce_sum | solution.py:73
  (216 shorter events, 70.6 us)
Async XLA Ops:
  6.5 32.3 %copy-start = (bf16[2048,512]{1,0:T(8,128)(2,1)S(1)}, bf16[2048,512]{1,0:T(8,128)(2,1)}, u32[]{:S(2)}) copy-start(bf16[2048,512]{1,0:T(8,128)(2,1)} %param.17) | copy-start | bytes 6291460
  6.5 32.3 %all-gather.10.cloned.1.call-start = ((), (), s32[]{:S(2)}) async-start(), calls=%async_computation.2 | async-start | bytes 3145728 | tf_op jit(solution)/shard_map/all_gather | solution.py:27
  6.5 2.4 %copy-start.6 = (bf16[512,2048]{1,0:T(8,128)(2,1)S(1)}, bf16[512,2048]{1,0:T(8,128)(2,1)}, u32[]{:S(2)}) copy-start(bf16[512,2048]{1,0:T(8,128)(2,1)} %param.15) | copy-start | bytes 6291460
  11.7 33.4 %all-gather.8.cloned.1.call-start = ((), (), s32[]{:S(2)}) async-start(), calls=%async_computation.1 | async-start | bytes 3145728 | tf_op jit(solution)/shard_map/all_gather | solution.py:27
  45.1 3.0 %copy-start.10 = (bf16[2,256,2560]{2,1,0:T(8,128)(2,1)S(1)}, bf16[2,256,2560]{2,1,0:T(8,128)(2,1)}, u32[]{:S(2)}) copy-start(bf16[2,256,2560]{2,1,0:T(8,128)(2,1)} %fusion.95) | copy-start | bytes 7864324
  45.1 3.0 %copy-start.38 = (bf16[2048,512]{1,0:T(8,128)(2,1)S(1)}, bf16[2048,512]{1,0:T(8,128)(2,1)}, u32[]{:S(2)}) copy-start(bf16[2048,512]{1,0:T(8,128)(2,1)} %param.18) | copy-start | bytes 6291460
  45.1 3.6 %copy-start.44 = (bf16[512,2048]{1,0:T(8,128)(2,1)S(1)}, bf16[512,2048]{1,0:T(8,128)(2,1)}, u32[]{:S(2)}) copy-start(bf16[512,2048]{1,0:T(8,128)(2,1)} %all-gather.10.cloned.1.call-done) | copy-start | bytes 6291460
  60.5 2.3 %copy-start.2 = (bf16[2,512,2560]{2,1,0:T(8,128)(2,1)}, bf16[2,512,2560]{2,1,0:T(8,128)(2,1)S(1)}, u32[]{:S(2)}) copy-start(bf16[2,512,2560]{2,1,0:T(8,128)(2,1)S(1)} %pad_maximum_fusion) | copy-start | bytes 15728644
  65.3 88.1 %collective-permute-start = (bf16[16,512]{0,1:T(8,128)(2,1)}, bf16[16,512]{0,1:T(8,128)(2,1)}, u32[]{:S(2)}, u32[]{:S(2)}) collective-permute-start(bf16[16,512]{0,1:T(8,128)(2,1)} %copy.57), channel_id=1, source_target_pairs={{0,8},{8,16},{16,24},{24,32},{32,40},{40,48},{48,56},{56,64},{64,7... | collective-permute-start | bytes 49160 | tf_op jit(solution)/shard_map/ppermute | solution.py:62
  72.1 1.8 copy-start.9
  77.1 2.6 %copy-start.3 = (f32[1024,4,64]{0,2,1:T(8,128)}, f32[1024,4,64]{0,2,1:T(8,128)S(1)}, u32[]{:S(2)}) copy-start(f32[1024,4,64]{0,2,1:T(8,128)S(1)} %get-tuple-element.238) | copy-start | bytes 3145732
  126.6 21.3 %copy-start.4 = (f32[1024,4,64]{0,2,1:T(8,128)S(1)}, f32[1024,4,64]{0,2,1:T(8,128)}, u32[]{:S(2)}) copy-start(f32[1024,4,64]{0,2,1:T(8,128)} %copy-done.3) | copy-start | bytes 3145732
  126.6 21.3 %copy-start.17 = (f32[4]{0:T(128)S(1)}, f32[4]{0:T(128)}, u32[]{:S(2)}) copy-start(f32[4]{0:T(128)} %get-tuple-element.247) | copy-start | bytes 52
  126.6 21.3 %copy-start.18 = (f32[4]{0:T(128)S(1)}, f32[4]{0:T(128)}, u32[]{:S(2)}) copy-start(f32[4]{0:T(128)} %get-tuple-element.249) | copy-start | bytes 52
  126.6 21.3 %copy-start.19 = (f32[4]{0:T(128)S(1)}, f32[4]{0:T(128)}, u32[]{:S(2)}) copy-start(f32[4]{0:T(128)} %get-tuple-element.250) | copy-start | bytes 52
  126.6 21.3 %copy-start.20 = (f32[4]{0:T(128)S(1)}, f32[4]{0:T(128)}, u32[]{:S(2)}) copy-start(f32[4]{0:T(128)} %get-tuple-element.251) | copy-start | bytes 52
  126.6 21.3 %copy-start.21 = (f32[4]{0:T(128)S(1)}, f32[4]{0:T(128)}, u32[]{:S(2)}) copy-start(f32[4]{0:T(128)} %fusion.212) | copy-start | bytes 52
  150.9 1.8 copy-start.8
  155.1 11.5 %copy-start.14 = (bf16[2,256,256]{2,1,0:T(8,128)(2,1)S(1)}, bf16[2,256,256]{2,1,0:T(8,128)(2,1)}, u32[]{:S(2)}) copy-start(bf16[2,256,256]{2,1,0:T(8,128)(2,1)} %param.22) | copy-start | bytes 786436
  155.1 11.5 %copy-start.15 = (f32[2,256]{1,0:T(2,128)S(1)}, f32[2,256]{1,0:T(2,128)}, u32[]{:S(2)}) copy-start(f32[2,256]{1,0:T(2,128)} %param.23) | copy-start | bytes 6148
  168.8 2.4 %copy-start.11 = (f32[1024,512]{1,0:T(8,128)S(1)}, f32[1024,512]{1,0:T(8,128)}, u32[]{:S(2)}) copy-start(f32[1024,512]{1,0:T(8,128)} %copy.48) | copy-start | bytes 6291460
  168.8 2.4 %copy-start.43 = (bf16[512,2048]{1,0:T(8,128)(2,1)S(1)}, bf16[512,2048]{1,0:T(8,128)(2,1)}, u32[]{:S(2)}) copy-start(bf16[512,2048]{1,0:T(8,128)(2,1)} %param.27) | copy-start | bytes 6291460
  168.8 2.4 %copy-start.46 = (f32[512]{0:T(512)S(1)}, f32[512]{0:T(512)}, u32[]{:S(2)}) copy-start(f32[512]{0:T(512)} %param.25) | copy-start | bytes 6148
  175.2 18.5 %copy-start.1 = (bf16[2048,512]{1,0:T(8,128)(2,1)S(1)}, bf16[2048,512]{1,0:T(8,128)(2,1)}, u32[]{:S(2)}) copy-start(bf16[2048,512]{1,0:T(8,128)(2,1)} %param.17) | copy-start | bytes 6291460
  (26 other events, 41.9 us)
Sparse Core Ops, SparseCore 0:
  11.9 16.8 all-gather.9
  30.5 14.6 all-gather.7
where the time goes:
time: 201 us; the launch traced here: 200 us
  blocking collectives  52.1 us (26%)
  local copies, waits for them, and re-layouts  49.3 us (25%)
  other arithmetic  38.9 us (19%)
  matrix products  38.2 us (19%)
  between operations  14.2 us (7%)
  starting transfers between devices  3.91 us (2%)
  waiting for transfers between devices  3.27 us (2%)
    all_gather x4, blocking collectives, carried_in(): lax.all_gather(part.astype(kind), axis)  38.8 us
    dynamic_slice x16, local copies, waits for them, and re-layouts, retain(): lax.scan(advance, start, (split(query), split(key), split(value)))  22.1 us
    dot_general x10, matrix products, project(): jnp.dot(piece, weight, preferred_element_type=jnp.float32)  16.8 us
    unnamed x102, local copies, waits for them, and re-layouts  14.8 us
    all_to_all x1, blocking collectives, sent_and_summed(): parts = lax.all_to_all(split_up(array, dim, length), axis, 0, 0, tiled=True)  13.4 us
    convert_element_type x1, other arithmetic, per_device(): diff = (window_sum / count - padded[rim_len:]).astype(jnp.bfloat16).resha...  11.4 us
    dot_general x8, matrix products, advance(): out = out + jnp.einsum('hid,hde->hie', qb, state) * query_decay[:, :, None]  7.15 us
    reduce_sum x1, other arithmetic, sent_and_summed(): return jnp.sum(parts.astype(jnp.float32), axis=0)  5.08 us
  transfers between devices with their start and end apart: 3, of which 1 were waited for; matrix products, arithmetic and copies ran while one was open for 37% of the time, Pallas kernels for 0%

commit v1 on v0

v1 whole, which is shorter than its diff:
```python
import functools

import jax
import jax.numpy as jnp
import numpy as np
from jax import lax
from jax.experimental import pallas as pl
from jax.experimental.pallas import tpu as pltpu
from jax.sharding import Mesh
from jax.sharding import PartitionSpec as P

f32 = jnp.float32
bf16 = jnp.bfloat16

GROUP_DIM = 256
HEAD_DIM = 128
CHUNK = 256
RIM = 16
EPS = 1e-06
SP = ("sp_0", "sp_1")
FS_SP_TP = ("fs", "sp_0", "sp_1", "tp")
LONG, SHORT = 32, 32


def mm(a, b):
    return lax.dot_general(a, b, (((1,), (0,)), ((), ())), preferred_element_type=f32)


def mm_t(a, b):
    return lax.dot_general(a, b, (((1,), (1,)), ((), ())), preferred_element_type=f32)


def t_mm(a, b):
    return lax.dot_general(a, b, (((0,), (0,)), ((), ())), preferred_element_type=f32)


def call(body, outs, ins, scratch, limit_mib, flops, args, name):
    vm = pl.BlockSpec(memory_space=pltpu.VMEM)
    any_ = pl.BlockSpec(memory_space=pl.ANY)
    nbytes = sum(int(np.prod(a.shape)) * a.dtype.itemsize for a in args)
    return pl.pallas_call(
        body,
        out_shape=outs,
        in_specs=[any_ if kind == "a" else vm for kind in ins],
        out_specs=jax.tree.map(lambda _: vm, outs),
        scratch_shapes=scratch,
        compiler_params=pltpu.CompilerParams(vmem_limit_bytes=limit_mib << 20),
        cost_estimate=pl.CostEstimate(flops=int(flops), bytes_accessed=nbytes, transcendentals=0),
        name=name,
    )(*args)


def sds(shape, dtype):
    return jax.ShapeDtypeStruct(shape, dtype)


class Dims:
    def __init__(self, rows, width, heads, total_heads, seq):
        self.rows, self.width, self.heads = rows, width, heads
        self.chunks = rows // CHUNK
        self.block = 2 * rows
        base = [-(2.0**-5) * (seq / 16.0) ** (-2.0 * h / (total_heads - 1)) for h in range(total_heads)]
        self.logd = [float(np.float32(v)) for v in base]

    def log_decay(self, tp, h):
        return jnp.where(tp == 0, f32(self.logd[h]), f32(self.logd[h + self.heads]))


def decay(l, steps):
    return jnp.exp(jnp.full((1, HEAD_DIM), l * steps, f32))


def normalize(x_ref, gain_ref, out_ref):
    rows = x_ref.shape[0]
    step = 16

    @pl.loop(0, rows // step, unroll=4)
    def _(i):
        at = pl.ds(pl.multiple_of(i * step, step), step)
        x = x_ref[at, :].astype(f32)
        ms = jnp.mean(x * x, axis=-1, keepdims=True)
        out_ref[at, :] = (x * lax.rsqrt(ms + EPS) * gain_ref[...]).astype(bf16)


def angle_tables(a_cos, a_sin, b_cos, b_sin, cos_ref, sin_ref):
    c2, s2 = b_cos[...], b_sin[...]
    for a in range(a_cos.shape[0]):
        c1, s1 = a_cos[a : a + 1, :], a_sin[a : a + 1, :]
        at = slice(a * SHORT, (a + 1) * SHORT)
        cos_ref[at, :] = c1 * c2 - s1 * s2
        sin_ref[at, :] = s1 * c2 + c1 * s2


def row_scale(l):
    steps = lax.broadcasted_iota(jnp.int32, (CHUNK, HEAD_DIM), 0).astype(f32)
    return jnp.exp(l * steps)


def rotate_heads(d, xn_ref, w_ref, cos_ref, sin_ref, tp, sign, scale, out_ref):
    for pair in range(d.heads // 2):
        cols = slice(pair * 2 * HEAD_DIM, (pair + 1) * 2 * HEAD_DIM)
        acc = mm(xn_ref[...], w_ref[:, cols])
        for hh in range(2):
            h = 2 * pair + hh
            x = acc[:, hh * HEAD_DIM : (hh + 1) * HEAD_DIM].astype(bf16).astype(f32)
            y = x * cos_ref[...] + pltpu.roll(x, HEAD_DIM // 2, 1) * sin_ref[...]
            r = row_scale(sign * d.log_decay(tp, h)) * scale
            for c in range(d.chunks):
                at = slice(c * CHUNK, (c + 1) * CHUNK)
                out_ref[at, h * HEAD_DIM : (h + 1) * HEAD_DIM] = (y[at] * r).astype(bf16)


def centering():
    i = lax.broadcasted_iota(jnp.int32, (2 * HEAD_DIM, 2 * HEAD_DIM), 0)
    j = lax.broadcasted_iota(jnp.int32, (2 * HEAD_DIM, 2 * HEAD_DIM), 1)
    same = (i // HEAD_DIM) == (j // HEAD_DIM)
    mean = jnp.where(same, f32(1.0 / HEAD_DIM), f32(0.0))
    return i, j, mean


def centred_values(d, xn_ref, w_ref, out_ref):
    i, j, mean = centering()
    keep = (jnp.where(i == j, f32(1.0), f32(0.0)) - mean).astype(bf16)
    for pair in range(d.heads // 2):
        cols = slice(pair * 2 * HEAD_DIM, (pair + 1) * 2 * HEAD_DIM)
        v = mm(xn_ref[...], w_ref[:, cols]).astype(bf16)
        out_ref[:, cols] = mm(v, keep).astype(bf16)


def chunk_states(d, k_ref, v_ref, tp, u_ref):
    for h in range(d.heads):
        cols = slice(h * HEAD_DIM, (h + 1) * HEAD_DIM)
        last = decay(d.log_decay(tp, h), CHUNK - 1.0)
        for c in range(d.chunks):
            at = slice(c * CHUNK, (c + 1) * CHUNK)
            u_ref[c, h] = t_mm(k_ref[at, cols], v_ref[at, cols]) * last


def inside_chunks(d, q_ref, k_ref, v_ref, o_ref):
    i = lax.broadcasted_iota(jnp.int32, (CHUNK, CHUNK), 0)
    j = lax.broadcasted_iota(jnp.int32, (CHUNK, CHUNK), 1)
    causal = i >= j
    for c in range(d.chunks):
        at = slice(c * CHUNK, (c + 1) * CHUNK)
        for h in range(d.heads):
            cols = slice(h * HEAD_DIM, (h + 1) * HEAD_DIM)
            s = jnp.where(causal, mm_t(q_ref[at, cols], k_ref[at, cols]), 0.0).astype(bf16)
            o_ref[at, cols] = mm(s, v_ref[at, cols])


def load(src, dst, sem):
    copy = pltpu.make_async_copy(src, dst, sem)
    copy.start()
    return copy


def own_rows(
    d, x_hbm, gain, tc, ts, bc, bs, wk_hbm, wv_hbm, wq_hbm,
    xn, q_out, u_out, o_out, x, wk, wv, wq, k, v, ac, as_, cos, sin, sems,
):
    tp = lax.axis_index("tp")
    sp = lax.axis_index("sp_0") * 4 + lax.axis_index("sp_1")
    n = d.rows // LONG
    first = pl.multiple_of((sp * 2 + tp) * n, n)
    cx = load(x_hbm, x, sems.at[0])
    c1 = load(tc.at[pl.ds(first, n)], ac, sems.at[1])
    c2 = load(ts.at[pl.ds(first, n)], as_, sems.at[2])
    ck = load(wk_hbm, wk, sems.at[3])
    cv = load(wv_hbm, wv, sems.at[4])
    cq = load(wq_hbm, wq, sems.at[5])
    c1.wait()
    c2.wait()
    angle_tables(ac, as_, bc, bs, cos, sin)
    cx.wait()
    normalize(x, gain, xn)
    ck.wait()
    rotate_heads(d, xn, wk, cos, sin, tp, -1.0, HEAD_DIM**-0.5, k)
    cv.wait()
    centred_values(d, xn, wv, v)
    chunk_states(d, k, v, tp, u_out)
    cq.wait()
    rotate_heads(d, xn, wq, cos, sin, tp, 1.0, 1.0, q_out)
    inside_chunks(d, q_out, k, v, o_out)


def partner_keys(
    d, x_hbm, gain, tc, ts, bc, bs, wk_hbm, wv_hbm, u_own,
    xn, k_out, v_out, u_out, s_out, cos, sin, x, wk, wv, ac, as_, sems,
):
    tp = lax.axis_index("tp")
    sp = lax.axis_index("sp_0") * 4 + lax.axis_index("sp_1")
    n = d.rows // LONG
    first = pl.multiple_of((sp * 2 + 1 - tp) * n, n)
    cx = load(x_hbm, x, sems.at[0])
    c1 = load(tc.at[pl.ds(first, n)], ac, sems.at[1])
    c2 = load(ts.at[pl.ds(first, n)], as_, sems.at[2])
    ck = load(wk_hbm, wk, sems.at[3])
    cv = load(wv_hbm, wv, sems.at[4])
    c1.wait()
    c2.wait()
    angle_tables(ac, as_, bc, bs, cos, sin)
    cx.wait()
    normalize(x, gain, xn)
    ck.wait()
    rotate_heads(d, xn, wk, cos, sin, tp, -1.0, HEAD_DIM**-0.5, k_out)
    cv.wait()
    centred_values(d, xn, wv, v_out)
    chunk_states(d, k_out, v_out, tp, u_out)
    last = 2 * d.chunks - 1
    for h in range(d.heads):
        l = d.log_decay(tp, h)
        total = jnp.zeros((HEAD_DIM, HEAD_DIM), f32)
        for c in range(d.chunks):
            own = (last - c - tp * d.chunks).astype(f32) * CHUNK
            other = (last - c - (1 - tp) * d.chunks).astype(f32) * CHUNK
            total += decay(l, own) * u_own[c, h] + decay(l, other) * u_out[c, h]
        s_out[h * HEAD_DIM : (h + 1) * HEAD_DIM, :] = total.astype(bf16)


def partner_queries(
    d, xn_own, xn_par, k, v, cos, sin, wp_hbm, wq_hbm,
    pool_out, tail_out, q_out, o_out, wp, wq, sems,
):
    tp = lax.axis_index("tp")
    cp = load(wp_hbm, wp, sems.at[0])
    cq = load(wq_hbm, wq, sems.at[1])
    own = pl.multiple_of(tp * d.rows, d.rows)
    other = pl.multiple_of((1 - tp) * d.rows, d.rows)
    cp.wait()
    for at, xn in ((own, xn_own), (other, xn_par)):
        for t in range(d.width // 256):
            cols = slice(t * 256, (t + 1) * 256)
            pool_out[pl.ds(at, d.rows), cols] = mm(xn[...], wp[:, cols]).astype(bf16)
    tail_out[...] = pool_out[d.block - RIM :, :]
    cq.wait()
    rotate_heads(d, xn_par, wq, cos, sin, tp, 1.0, 1.0, q_out)
    inside_chunks(d, q_out, k, v, o_out)


def row_states(d, own, r1, r2, r3, total_out, prefix_out):
    tp = lax.axis_index("tp")
    y = lax.axis_index("sp_1")
    for h in range(d.heads):
        at = slice(h * HEAD_DIM, (h + 1) * HEAD_DIM)
        l = d.log_decay(tp, h)
        total = decay(l, (3 - y).astype(f32) * d.block) * own[at, :].astype(f32)
        prefix = jnp.zeros((HEAD_DIM, HEAD_DIM), f32)
        for k, r in ((1, r1), (2, r2), (3, r3)):
            part = r[at, :].astype(f32)
            behind = lax.rem(y - k + 4, 4)
            total += decay(l, (3 - behind).astype(f32) * d.block) * part
            prefix += jnp.where(y >= k, decay(l, (k - 1.0) * d.block), 0.0) * part
        total_out[at, :] = total.astype(bf16)
        prefix_out[at, :] = prefix


def gates_and_pools(
    d, xn_own, xn_par, pool_in, rim, mix, bias, gain, ret_gain, wg_hbm,
    g_own, g_par, p_own, p_par, wg, ext, po, sems,
):
    tp = lax.axis_index("tp")
    sp = lax.axis_index("sp_0") * 4 + lax.axis_index("sp_1")
    cg = load(wg_hbm, wg, sems.at[0])
    own = pl.multiple_of(tp * d.rows, d.rows)
    other = pl.multiple_of((1 - tp) * d.rows, d.rows)
    ext[0:RIM, :] = rim[...]
    ext[RIM:, :] = pool_in[...]
    i = lax.broadcasted_iota(jnp.int32, (CHUNK, CHUNK + RIM), 0) + RIM
    j = lax.broadcasted_iota(jnp.int32, (CHUNK, CHUNK + RIM), 1)
    groups = d.width // GROUP_DIM
    for g in range(groups):
        window = jnp.where(tp == 0, 2 ** (g + 1), 2 ** (g + 1 + groups))
        band = jnp.where((i >= j) & (i - j < window), f32(1.0), f32(0.0)).astype(bf16)
        cols = slice(g * GROUP_DIM, (g + 1) * GROUP_DIM)
        for c in range(2 * d.chunks):
            rows = slice(c * CHUNK, (c + 1) * CHUNK)
            t = lax.broadcasted_iota(jnp.int32, (CHUNK, 1), 0) + (sp * d.block + c * CHUNK + 1)
            count = jnp.minimum(t, window).astype(f32)
            sums = mm(band, ext[c * CHUNK : c * CHUNK + CHUNK + RIM, cols])
            diff = sums * (1.0 / count) - pool_in[rows, cols].astype(f32)
            mixed = mm(diff.astype(bf16), mix[g]) + bias[g : g + 1, :]
            po[rows, cols] = (mixed * gain[:, cols]).astype(bf16)
    p_own[...] = po[pl.ds(own, d.rows), :]
    p_par[...] = po[pl.ds(other, d.rows), :]
    cg.wait()
    for xn, out in ((xn_own, g_own), (xn_par, g_par)):
        for t in range(d.width // 256):
            cols = slice(t * 256, (t + 1) * 256)
            gate = mm(xn[...], wg[:, cols]).astype(bf16).astype(f32)
            out[:, cols] = (gate * jax.nn.sigmoid(gate) * ret_gain[:, cols]).astype(bf16)


def retention_rows(d, half, tp, q, o, gate, prefix, z1, z2, z3, u_own, u_par, out, s_ref):
    z = lax.axis_index("sp_0")
    y = lax.axis_index("sp_1")
    rowlen = 4.0 * d.block
    s_ref[...] = jnp.zeros_like(s_ref)
    for h in range(d.heads):
        at = slice(h * HEAD_DIM, (h + 1) * HEAD_DIM)
        l = d.log_decay(tp, h)
        rows_before = jnp.zeros((HEAD_DIM, HEAD_DIM), f32)
        for k, r in ((1, z1), (2, z2), (3, z3)):
            rows_before += jnp.where(z >= k, decay(l, (k - 1.0) * rowlen), 0.0) * r[at, :].astype(f32)
        incoming = prefix[at, :] + decay(l, y.astype(f32) * d.block) * rows_before
        sub = slice((h % 2) * HEAD_DIM, (h % 2 + 1) * HEAD_DIM)
        one = decay(l, 1.0)
        step = decay(l, float(CHUNK))
        after = incoming
        for c in range(d.chunks):
            u_first = jnp.where(tp == 0, u_own[c, h], u_par[c, h])
            after = step * after + u_first
        state = jnp.where(half == 0, incoming, after)
        for c in range(d.chunks):
            s_ref[c, h // 2, sub, sub] = (one * state).astype(bf16)
            if c + 1 < d.chunks:
                u_here = jnp.where(half == tp, u_own[c, h], u_par[c, h])
                state = step * state + u_here
    _, _, mean = centering()
    mean = mean.astype(bf16)
    for c in range(d.chunks):
        at = slice(c * CHUNK, (c + 1) * CHUNK)
        for pair in range(d.heads // 2):
            cols = slice(pair * 2 * HEAD_DIM, (pair + 1) * 2 * HEAD_DIM)
            raw = o[at, cols] + mm(q[at, cols], s_ref[c, pair])
            var = mm((raw * raw).astype(bf16), mean)
            ret = gate[at, cols].astype(f32) * (raw * lax.rsqrt(var + EPS))
            out[at, cols] = ret.astype(bf16)


def partner_retention(d, q, o, gate, prefix, z1, z2, z3, u_own, u_par, out, s_ref):
    tp = lax.axis_index("tp")
    retention_rows(d, 1 - tp, tp, q, o, gate, prefix, z1, z2, z3, u_own, u_par, out, s_ref)


def pool_outputs(d, p_own, p_recv, w_own_hbm, w_par_hbm, acc, w_own, w_par, sems):
    co = load(w_own_hbm, w_own, sems.at[0])
    cp = load(w_par_hbm, w_par, sems.at[1])
    co.wait()
    cp.wait()
    for t in range(acc.shape[1] // 256):
        cols = slice(t * 256, (t + 1) * 256)
        acc[:, cols] = mm(p_own[...], w_own[:, cols]) + mm(p_recv[...], w_par[:, cols])


def own_retention(
    d, q, o, gate, prefix, z1, z2, z3, u_own, u_par, acc_in, w_hbm, acc, s_ref, ret, w, sems
):
    tp = lax.axis_index("tp")
    cw = load(w_hbm, w, sems.at[0])
    retention_rows(d, tp, tp, q, o, gate, prefix, z1, z2, z3, u_own, u_par, ret, s_ref)
    cw.wait()
    for t in range(acc.shape[1] // 256):
        cols = slice(t * 256, (t + 1) * 256)
        acc[:, cols] = acc_in[:, cols] + mm(ret[...], w[:, cols])


def last_share(d, acc_in, ret, w_hbm, out, w, sems):
    cw = load(w_hbm, w, sems.at[0])
    cw.wait()
    for t in range(out.shape[1] // 256):
        cols = slice(t * 256, (t + 1) * 256)
        out[:, cols] = (acc_in[:, cols] + mm(ret[...], w[:, cols])).astype(bf16)


def swap(x):
    return lax.ppermute(x, "tp", [(0, 1), (1, 0)])


def per_device(
    seq, tokens, norm_gain, w_pool, w_query, w_key, w_value, w_gate, pool_mix, pool_bias,
    pool_gain, ret_gain, w_out_pool, w_out_ret,
):
    rows, model = tokens.shape
    width = w_query.shape[1]
    heads = width // HEAD_DIM
    d = Dims(rows, width, heads, heads * 2, seq)
    n = rows // LONG
    dma = pltpu.SemaphoreType.DMA
    vmem = pltpu.VMEM
    gain = norm_gain[None, :]

    half = HEAD_DIM // 2
    freq = 10000.0 ** (-np.arange(half, dtype=np.float64) / half)
    freq = np.concatenate([freq, freq])
    sign = np.concatenate([-np.ones(half), np.ones(half)])
    a = np.arange(seq // LONG)[:, None] * float(LONG) * freq
    b = np.arange(SHORT)[:, None] * freq
    tc, ts = np.cos(a).astype(np.float32), (np.sin(a) * sign).astype(np.float32)
    bc, bs = np.cos(b).astype(np.float32), (np.sin(b) * sign).astype(np.float32)

    proj = 2.0 * rows * model * width
    other_tokens = swap(tokens)
    u_shape = sds((d.chunks, heads, HEAD_DIM, HEAD_DIM), f32)
    act = sds((rows, width), bf16)
    xn_own, q_own, u_own, o_own = call(
        functools.partial(own_rows, d),
        [sds((rows, model), bf16), act, u_shape, sds((rows, width), f32)],
        "avaavvaaa",
        [
            vmem((rows, model), bf16), vmem((model, width), bf16), vmem((model, width), bf16),
            vmem((model, width), bf16), vmem((rows, width), bf16), vmem((rows, width), bf16),
            vmem((n, HEAD_DIM), f32), vmem((n, HEAD_DIM), f32), vmem((rows, HEAD_DIM), f32),
            vmem((rows, HEAD_DIM), f32), dma((6,)),
        ],
        28, 3.6 * proj, (tokens, gain, tc, ts, bc, bs, w_key, w_value, w_query), "own_rows",
    )
    other_pool_w = swap(w_out_pool)
    other_ret_w = swap(w_out_ret)
    xn_par, k_par, v_par, u_par, state, cos, sin = call(
        functools.partial(partner_keys, d),
        [
            sds((rows, model), bf16), act, act, u_shape, sds((width, HEAD_DIM), bf16),
            sds((rows, HEAD_DIM), f32), sds((rows, HEAD_DIM), f32),
        ],
        "avaavvaav",
        [
            vmem((rows, model), bf16), vmem((model, width), bf16), vmem((model, width), bf16),
            vmem((n, HEAD_DIM), f32), vmem((n, HEAD_DIM), f32), dma((5,)),
        ],
        24, 2.4 * proj, (other_tokens, gain, tc, ts, bc, bs, w_key, w_value, u_own), "partner_keys",
    )
    ys = [lax.ppermute(state, "sp_1", [(i, (i + k) % 4) for i in range(4)]) for k in (1, 2, 3)]
    pool_in, tail, q_par, o_par = call(
        functools.partial(partner_queries, d),
        [sds((d.block, width), bf16), sds((RIM, width), bf16), act, sds((rows, width), f32)],
        "vvvvvvaa",
        [vmem((model, width), bf16), vmem((model, width), bf16), dma((2,))],
        24, 3.4 * proj, (xn_own, xn_par, k_par, v_par, cos, sin, w_pool, w_query), "partner_queries",
    )
    rim = lax.ppermute(tail, SP, [(i, i + 1) for i in range(seq // d.block - 1)])
    total, prefix = call(
        functools.partial(row_states, d),
        [sds((width, HEAD_DIM), bf16), sds((width, HEAD_DIM), f32)],
        "vvvv", [], 4, 0.1 * proj, (state, *ys), "row_states",
    )
    zs = [lax.ppermute(total, "sp_0", [(i, i + k) for i in range(4 - k)]) for k in (1, 2, 3)]
    g_own, g_par, p_own, p_par = call(
        functools.partial(gates_and_pools, d),
        [act, act, act, act],
        "vvvvvvvva",
        [
            vmem((model, width), bf16), vmem((d.block + RIM, width), bf16),
            vmem((d.block, width), bf16), dma((1,)),
        ],
        24, 2.8 * proj,
        (xn_own, xn_par, pool_in, rim, pool_mix, pool_bias, pool_gain[None], ret_gain[None], w_gate),
        "gates_and_pools",
    )
    p_recv = swap(p_par)
    acc = call(
        functools.partial(pool_outputs, d),
        sds((rows, model), f32), "vvaa",
        [vmem((width, model), bf16), vmem((width, model), bf16), dma((2,))],
        16, 2.0 * proj, (p_own, p_recv, w_out_pool, other_pool_w), "pool_outputs",
    )
    s_scratch = vmem((d.chunks, heads // 2, 2 * HEAD_DIM, 2 * HEAD_DIM), bf16)
    ret_par = call(
        functools.partial(partner_retention, d),
        act, "vvvvvvvvv", [s_scratch], 12, 0.5 * proj,
        (q_par, o_par, g_par, prefix, *zs, u_own, u_par), "partner_retention",
    )
    ret_recv = swap(ret_par)
    acc = call(
        functools.partial(own_retention, d),
        sds((rows, model), f32), "vvvvvvvvvva",
        [s_scratch, vmem((rows, width), bf16), vmem((width, model), bf16), dma((1,))],
        20, 1.5 * proj,
        (q_own, o_own, g_own, prefix, *zs, u_own, u_par, acc, w_out_ret), "own_retention",
    )
    return call(
        functools.partial(last_share, d),
        sds((rows, model), bf16), "vva",
        [vmem((width, model), bf16), dma((1,))],
        16, 1.0 * proj, (acc, ret_recv, other_ret_w), "last_share",
    )


def solution(mesh):
    finer = Mesh(
        mesh.devices.reshape(4, 4, mesh.shape["fs"], mesh.shape["tp"]), ("sp_0", "sp_1", "fs", "tp")
    )
    placed = (
        P(FS_SP_TP, None), P(), P(None, "tp"), P(None, "tp"), P(None, "tp"), P(None, "tp"),
        P(None, "tp"), P("tp", None, None), P("tp", None), P("tp"), P("tp"), P("tp", None),
        P("tp", None),
    )

    def whole(tokens, *rest):
        seq = tokens.shape[0] // mesh.shape["fs"]
        return jax.shard_map(
            functools.partial(per_device, seq), mesh=finer, in_specs=placed,
            out_specs=P(FS_SP_TP, None), check_vma=False,
        )(tokens, *rest)

    return whole
```

time: 201 us -> 71.7 us (0.36)
  blocking collectives: 52.1 us -> 0 us
  other arithmetic: 38.9 us -> 0 us
  local copies, waits for them, and re-layouts: 49.3 us -> 10.5 us
  matrix products: 38.2 us -> 0 us
  Pallas kernels: 0 us -> 32.8 us
  starting transfers between devices: 3.91 us -> 25.6 us
  between operations: 14.2 us -> 0.44 us
    all_gather x4 -> x0, blocking collectives: 38.8 us -> none  [carried_in(): lax.all_gather(part.astype(kind), axis)]
    dot_general x38 -> x0, matrix products: 38.2 us -> none  [the longest x10 16.8 us: project(): jnp.dot(piece, weight, preferred_element_type=jnp.float32)]
    pallas_call x0 -> x9, Pallas kernels: none -> 32.8 us  [call(): pl.pallas_call(body, out_shape=outs, in_specs=[any_ if kind == 'a' else v...]
    dynamic_slice x16 -> x0, local copies, waits for them, and re-layouts: 22.1 us -> none  [retain(): lax.scan(advance, start, (split(query), split(key), split(value)))]
    ppermute x1 -> x12, starting transfers between devices: 3.87 us -> 25.6 us  [the longest x3 12.6 us: per_device(): lax.ppermute(total, 'sp_0', [(i, i + k) for i in range(4 - k)])]
    convert_element_type x10 -> x0, other arithmetic: 15.1 us -> none  [the longest x1 11.4 us: per_device(): diff = (window_sum / count - padded[rim_len:]).astype(jnp.bfloat16).resha...]
    all_to_all x1 -> x0, blocking collectives: 13.4 us -> none  [sent_and_summed(): parts = lax.all_to_all(split_up(array, dim, length), axis, 0, 0, tiled=True)]
    reduce_sum x3 -> x0, other arithmetic: 7.58 us -> none  [the longest x1 5.08 us: sent_and_summed(): return jnp.sum(parts.astype(jnp.float32), axis=0)]
  transfers between devices with their start and end apart: 3 -> 12, of which waited for: 1 -> 1; matrix products, arithmetic and copies ran while one was open for 37% -> 0% of each run, Pallas kernels for 0% -> 42%
where the time goes in v1:
time: 71.7 us; the launch traced here: 71.2 us
  Pallas kernels  32.8 us (46%)
  starting transfers between devices  25.6 us (36%)
  local copies, waits for them, and re-layouts  10.5 us (15%)
  waiting for transfers between devices  1.94 us (3%)
    pallas_call x9, Pallas kernels, call(): pl.pallas_call(body, out_shape=outs, in_specs=[any_ if kind == 'a' else v...  32.8 us
    ppermute x3, starting transfers between devices, per_device(): lax.ppermute(total, 'sp_0', [(i, i + k) for i in range(4 - k)])  12.6 us
    unnamed x40, local copies, waits for them, and re-layouts  10.5 us
    ppermute x5, starting transfers between devices, swap(): return lax.ppermute(x, 'tp', [(0, 1), (1, 0)])  4.94 us
    ppermute x3, starting transfers between devices, per_device(): lax.ppermute(state, 'sp_1', [(i, (i + k) % 4) for i in range(4)])  4.76 us
    ppermute x1, starting transfers between devices, per_device(): lax.ppermute(tail, SP, [(i, i + 1) for i in range(seq // d.block - 1)])  3.32 us
    ppermute x3, waiting for transfers between devices, per_device(): lax.ppermute(total, 'sp_0', [(i, i + k) for i in range(4 - k)])  1.92 us
  transfers between devices with their start and end apart: 12, of which 1 were waited for; matrix products, arithmetic and copies ran while one was open for 0% of the time, Pallas kernels for 42%

profile of v1, /device:TPU:1, one launch (start us, length us, event | category | flops | bytes accessed | tf_op | source)
XLA Modules:
  0.0 71.2 jit_solution(5645304330624982267)
XLA Ops:
  0.0 1.4 %collective-permute-start = (bf16[512,2048]{1,0:T(8,128)(2,1)}, bf16[512,2048]{1,0:T(8,128)(2,1)S(1)}, u32[]{:S(2)}, u32[]{:S(2)}) collective-permute-start(bf16[512,2048]{1,0:T(8,128)(2,1)} %x_hbm.1), channel_id=1, source_target_pairs={{0,1},{1,0},{2,3},{3,2},{4,5},{5,4},{6,7},{7,6},{8,9},{9,8},{10,11... | collective-permute-start | bytes 6291464 | tf_op jit(solution)/shard_map/ppermute | solution.py:366
  1.9 1.6 %copy-done.2 = bf16[512,2048]{1,0:T(8,128)(2,1)S(1)} copy-done((bf16[512,2048]{1,0:T(8,128)(2,1)S(1)}, bf16[512,2048]{1,0:T(8,128)(2,1)}, u32[]{:S(2)}) %copy-start.2) | copy-done | bytes 2097176
  3.5 1.6 %copy-done.3 = bf16[2048,512]{1,0:T(8,128)(2,1)S(1)} copy-done((bf16[2048,512]{1,0:T(8,128)(2,1)S(1)}, bf16[2048,512]{1,0:T(8,128)(2,1)}, u32[]{:S(2)}) %copy-start.3) | copy-done | bytes 2097176
  5.1 1.6 %copy-done.5 = bf16[2048,512]{1,0:T(8,128)(2,1)S(1)} copy-done((bf16[2048,512]{1,0:T(8,128)(2,1)S(1)}, bf16[2048,512]{1,0:T(8,128)(2,1)}, u32[]{:S(2)}) %copy-start.5) | copy-done | bytes 2097176
  6.7 1.6 %copy-done.7 = bf16[2048,512]{1,0:T(8,128)(2,1)S(1)} copy-done((bf16[2048,512]{1,0:T(8,128)(2,1)S(1)}, bf16[2048,512]{1,0:T(8,128)(2,1)}, u32[]{:S(2)}) %copy-start.7) | copy-done | bytes 2097176
  9.0 0.9 %copy-done.16 = f32[512,128]{1,0:T(8,128)S(1)} copy-done((f32[512,128]{1,0:T(8,128)S(1)}, f32[512,128]{1,0:T(8,128)}, u32[]{:S(2)}) %copy-start.16) | copy-done | bytes 262168
  9.9 0.9 %copy-done.17 = f32[512,128]{1,0:T(8,128)S(1)} copy-done((f32[512,128]{1,0:T(8,128)S(1)}, f32[512,128]{1,0:T(8,128)}, u32[]{:S(2)}) %copy-start.17) | copy-done | bytes 262168
  12.3 8.3 %own_rows.1 = (bf16[512,2048]{1,0:T(8,128)(2,1)S(1)}, bf16[512,512]{1,0:T(8,128)(2,1)S(1)}, f32[2,4,128,128]{3,2,1,0:T(8,128)S(1)}, f32[512,512]{1,0:T(8,128)S(1)}) custom-call(bf16[512,2048]{1,0:T(8,128)(2,1)S(1)} %copy-done.2, f32[1,2048]{1,0:T(1,128)S(1)} %bitcast.3, f32[512,128]{1,0:T(8,128)S(1)} %copy-done.16, f32[512,128]{1,0:T(8,128)S(1)} %copy-done.17, ...), custom_call_target="tpu_custom_call" | custom-call | flops 3865470464 | bytes 8953856 | tf_op jit(solution)/shard_map/own_rows/pallas_call | solution.py:41
  20.7 6.1 %partner_keys.1 = (bf16[512,2048]{1,0:T(8,128)(2,1)S(1)}, bf16[512,512]{1,0:T(8,128)(2,1)S(1)}, bf16[512,512]{1,0:T(8,128)(2,1)S(1)}, f32[2,4,128,128]{3,2,1,0:T...) custom-call(bf16[512,2048]{1,0:T(8,128)(2,1)S(1)} %collective-permute-done.x_hbm, ...), custom_call_target="tpu_custom_call" | custom-call | flops 2576980480 | bytes 7380992 | tf_op jit(solution)/shard_map/partner_keys/pallas_call | solution.py:41
  26.9 4.8 %partner_queries.1 = (bf16[1024,512]{1,0:T(8,128)(2,1)S(1)}, bf16[16,512]{1,0:T(8,128)(2,1)S(1)}, bf16[512,512]{1,0:T(8,128)(2,1)S(1)}, f32[512,512]{1,0:T(8,128)S(1)}) custom-call(bf16[512,2048]{1,0:T(8,128)(2,1)S(1)} %get-tuple-element.28.xn_own, bf16[512,2048]{1,0:T(8,128)(2,1)S(1)} %get-tuple-element.30.xn_par, ...), custom_call_target="tpu_custom_call" | custom-call | flops 3650722304 | bytes 9961472 | tf_op jit(solution)/shard_map/partner_queries/pallas_call | solution.py:41
  31.7 3.3 %collective-permute-start.1 = (bf16[16,512]{1,0:T(8,128)(2,1)S(1)}, bf16[16,512]{1,0:T(8,128)(2,1)S(1)}, u32[]{:S(2)}, u32[]{:S(2)}) collective-permute-start(bf16[16,512]{1,0:T(8,128)(2,1)S(1)} %get-tuple-element.36), channel_id=1, source_target_pairs={{0,8},{8,16},{16,24},{24,32},{32,40},{40,48},{48,56},{56,64},{64,7... | collective-permute-start | bytes 49160 | tf_op jit(solution)/shard_map/ppermute | solution.py:430
  35.0 1.4 %collective-permute-start.2 = (bf16[512,128]{1,0:T(8,128)(2,1)S(1)}, bf16[512,128]{1,0:T(8,128)(2,1)S(1)}, u32[]{:S(2)}, u32[]{:S(2)}) collective-permute-start(bf16[512,128]{1,0:T(8,128)(2,1)S(1)} %get-tuple-element.38.own), channel_id=1, source_target_pairs={{0,8},{8,16},{16,24},{24,0},{1,9},{9,17},{17,25},{25,1},{2,10},{10... | collective-permute-start | bytes 393224 | tf_op jit(solution)/shard_map/ppermute | solution.py:422
  36.4 2.6 %collective-permute-start.3 = (bf16[512,128]{1,0:T(8,128)(2,1)S(1)}, bf16[512,128]{1,0:T(8,128)(2,1)S(1)}, u32[]{:S(2)}, u32[]{:S(2)}) collective-permute-start(bf16[512,128]{1,0:T(8,128)(2,1)S(1)} %get-tuple-element.38.own), channel_id=1, source_target_pairs={{0,16},{8,24},{16,0},{24,8},{1,17},{9,25},{17,1},{25,9},{2,18},{10... | collective-permute-start | bytes 393224 | tf_op jit(solution)/shard_map/ppermute | solution.py:422
  39.0 0.8 %collective-permute-start.4 = (bf16[512,128]{1,0:T(8,128)(2,1)S(1)}, bf16[512,128]{1,0:T(8,128)(2,1)S(1)}, u32[]{:S(2)}, u32[]{:S(2)}) collective-permute-start(bf16[512,128]{1,0:T(8,128)(2,1)S(1)} %get-tuple-element.38.own), channel_id=1, source_target_pairs={{0,24},{8,0},{16,8},{24,16},{1,25},{9,1},{17,9},{25,17},{2,26},{10... | collective-permute-start | bytes 393224 | tf_op jit(solution)/shard_map/ppermute | solution.py:422
  39.8 5.1 %gates_and_pools.1 = (bf16[512,512]{1,0:T(8,128)(2,1)S(1)}, bf16[512,512]{1,0:T(8,128)(2,1)S(1)}, bf16[512,512]{1,0:T(8,128)(2,1)S(1)}, bf16[512,512]{1,0:T(8,128)(2,1)S(1)}) custom-call(bf16[512,2048]{1,0:T(8,128)(2,1)S(1)} %get-tuple-element.28.xn_own, bf16[512,2048]{1,0:T(8,128)(2,1)S(1)} %get-tuple-element.30.xn_par, ...), custom_call_target="tpu_custom_call" | custom-call | flops 3006477056 | bytes 7624704 | tf_op jit(solution)/shard_map/gates_and_pools/pallas_call | solution.py:41
  44.9 1.2 %collective-permute-start.8 = (bf16[512,512]{1,0:T(8,128)(2,1)S(1)}, bf16[512,512]{1,0:T(8,128)(2,1)S(1)}, u32[]{:S(2)}, u32[]{:S(2)}) collective-permute-start(bf16[512,512]{1,0:T(8,128)(2,1)S(1)} %get-tuple-element.43), channel_id=1, source_target_pairs={{0,1},{1,0},{2,3},{3,2},{4,5},{5,4},{6,7},{7,6},{8,9},{9,8},{10,11... | collective-permute-start | bytes 1572872 | tf_op jit(solution)/shard_map/ppermute | solution.py:366
  46.3 3.6 %collective-permute-start.5 = (bf16[512,128]{1,0:T(8,128)(2,1)S(1)}, bf16[512,128]{1,0:T(8,128)(2,1)S(1)}, u32[]{:S(2)}, u32[]{:S(2)}) collective-permute-start(bf16[512,128]{1,0:T(8,128)(2,1)S(1)} %get-tuple-element.40), channel_id=1, source_target_pairs={{0,32},{32,64},{64,96},{1,33},{33,65},{65,97},{2,34},{34,66},{66,9... | collective-permute-start | bytes 393224 | tf_op jit(solution)/shard_map/ppermute | solution.py:436
  49.9 5.2 %collective-permute-start.6 = (bf16[512,128]{1,0:T(8,128)(2,1)S(1)}, bf16[512,128]{1,0:T(8,128)(2,1)S(1)}, u32[]{:S(2)}, u32[]{:S(2)}) collective-permute-start(bf16[512,128]{1,0:T(8,128)(2,1)S(1)} %get-tuple-element.40), channel_id=1, source_target_pairs={{0,64},{32,96},{1,65},{33,97},{2,66},{34,98},{3,67},{35,99},{4,68}... | collective-permute-start | bytes 393224 | tf_op jit(solution)/shard_map/ppermute | solution.py:436
  55.1 3.8 %collective-permute-start.7 = (bf16[512,128]{1,0:T(8,128)(2,1)S(1)}, bf16[512,128]{1,0:T(8,128)(2,1)S(1)}, u32[]{:S(2)}, u32[]{:S(2)}) collective-permute-start(bf16[512,128]{1,0:T(8,128)(2,1)S(1)} %get-tuple-element.40), channel_id=1, source_target_pairs={{0,96},{1,97},{2,98},{3,99},{4,100},{5,101},{6,102},{7,103},{8,104... | collective-permute-start | bytes 393224 | tf_op jit(solution)/shard_map/ppermute | solution.py:436
  58.9 1.9 %collective-permute-done.7.z3 = bf16[512,128]{1,0:T(8,128)(2,1)S(1)} collective-permute-done((bf16[512,128]{1,0:T(8,128)(2,1)S(1)}, bf16[512,128]{1,0:T(8,128)(2,1)S(1)}, u32[]{:S(2)}, u32[]{:S(2)}) %collective-permute-start.7) | collective-permute-done | bytes 131104 | tf_op jit(solution)/shard_map/ppermute | solution.py:436
  61.6 1.8 %collective-permute-start.10 = (bf16[512,512]{1,0:T(8,128)(2,1)S(1)}, bf16[512,512]{1,0:T(8,128)(2,1)S(1)}, u32[]{:S(2)}, u32[]{:S(2)}) collective-permute-start(bf16[512,512]{1,0:T(8,128)(2,1)S(1)} %partner_retention.1), channel_id=1, source_target_pairs={{0,1},{1,0},{2,3},{3,2},{4,5},{5,4},{6,7},{7,6},{8,9},{9,8},{10,11... | collective-permute-start | bytes 1572872 | tf_op jit(solution)/shard_map/ppermute | solution.py:366
  63.4 2.7 %pool_outputs.1.acc_in = f32[512,2048]{1,0:T(8,128)S(1)} custom-call(bf16[512,512]{1,0:T(8,128)(2,1)S(1)} %get-tuple-element.42.p_own, bf16[512,512]{1,0:T(8,128)(2,1)S(1)} %collective-permute-done.8.p_recv, bf16[512,2048]{1,0:T(8,128)(2,1)S(1)} %copy-done.1, bf16[512,2048]{1,0:T(8,128)(2,1)S(1)} %collective-permute-done.9.w_par_hbm), custom_call_target="tpu_custom_call" | custom-call | flops 2147483648 | bytes 5242880 | tf_op jit(solution)/shard_map/pool_outputs/pallas_call | solution.py:41
  66.1 2.2 %own_retention.1.acc_in = f32[512,2048]{1,0:T(8,128)S(1)} custom-call(bf16[512,512]{1,0:T(8,128)(2,1)S(1)} %get-tuple-element.26.q, f32[512,512]{1,0:T(8,128)S(1)} %get-tuple-element.27.o, bf16[512,512]{1,0:T(8,128)(2,1)S(1)} %get-tuple-element.37.gate, f32[512,128]{1,0:T(8,128)S(1)} %get-tuple-element.39.prefix, ...), custom_call_target="tpu_custom_call" | custom-call | flops 1610612736 | bytes 10092544 | tf_op jit(solution)/shard_map/own_retention/pallas_call | solution.py:41
  68.3 2.7 %last_share.1 = bf16[512,2048]{1,0:T(8,128)(2,1)} custom-call(f32[512,2048]{1,0:T(8,128)S(1)} %own_retention.1.acc_in, bf16[512,512]{1,0:T(8,128)(2,1)S(1)} %collective-permute-done.10.ret, bf16[512,2048]{1,0:T(8,128)(2,1)S(1)} %collective-permute-done.11.w_hbm), custom_call_target="tpu_custom_call" | custom-call | flops 1073741824 | bytes 6815744 | tf_op jit(solution)/shard_map/last_share/pallas_call | solution.py:41
  (49 shorter events, 3.7 us)
Async XLA Ops:
  0.0 20.7 %collective-permute-start = (bf16[512,2048]{1,0:T(8,128)(2,1)}, bf16[512,2048]{1,0:T(8,128)(2,1)S(1)}, u32[]{:S(2)}, u32[]{:S(2)}) collective-permute-start(bf16[512,2048]{1,0:T(8,128)(2,1)} %x_hbm.1), channel_id=1, source_target_pairs={{0,1},{1,0},{2,3},{3,2},{4,5},{5,4},{6,7},{7,6},{8,9},{9,8},{10,11... | collective-permute-start | bytes 6291464 | tf_op jit(solution)/shard_map/ppermute | solution.py:366
  1.4 62.0 %collective-permute-start.9 = (bf16[512,2048]{1,0:T(8,128)(2,1)}, bf16[512,2048]{1,0:T(8,128)(2,1)S(1)}, u32[]{:S(2)}, u32[]{:S(2)}) collective-permute-start(bf16[512,2048]{1,0:T(8,128)(2,1)} %w_own_hbm.1), channel_id=1, source_target_pairs={{0,1},{1,0},{2,3},{3,2},{4,5},{5,4},{6,7},{7,6},{8,9},{9,8},{10,11... | collective-permute-start | bytes 6291464 | tf_op jit(solution)/shard_map/ppermute | solution.py:366
  1.4 66.9 %collective-permute-start.11 = (bf16[512,2048]{1,0:T(8,128)(2,1)}, bf16[512,2048]{1,0:T(8,128)(2,1)S(1)}, u32[]{:S(2)}, u32[]{:S(2)}) collective-permute-start(bf16[512,2048]{1,0:T(8,128)(2,1)} %w_hbm.1), channel_id=1, source_target_pairs={{0,1},{1,0},{2,3},{3,2},{4,5},{5,4},{6,7},{7,6},{8,9},{9,8},{10,11... | collective-permute-start | bytes 6291464 | tf_op jit(solution)/shard_map/ppermute | solution.py:366
  3.5 1.6 %copy-start.3 = (bf16[2048,512]{1,0:T(8,128)(2,1)S(1)}, bf16[2048,512]{1,0:T(8,128)(2,1)}, u32[]{:S(2)}) copy-start(bf16[2048,512]{1,0:T(8,128)(2,1)} %wk_hbm.3) | copy-start | bytes 6291460
  12.3 8.4 %copy-start.4 = (bf16[2048,512]{1,0:T(8,128)(2,1)S(1)}, bf16[2048,512]{1,0:T(8,128)(2,1)}, u32[]{:S(2)}) copy-start(bf16[2048,512]{1,0:T(8,128)(2,1)} %wk_hbm.3) | copy-start | bytes 6291460
  12.3 8.4 %copy-start.6 = (bf16[2048,512]{1,0:T(8,128)(2,1)S(1)}, bf16[2048,512]{1,0:T(8,128)(2,1)}, u32[]{:S(2)}) copy-start(bf16[2048,512]{1,0:T(8,128)(2,1)} %wv_hbm.3) | copy-start | bytes 6291460
  20.7 6.1 %copy-start.8 = (bf16[2048,512]{1,0:T(8,128)(2,1)S(1)}, bf16[2048,512]{1,0:T(8,128)(2,1)}, u32[]{:S(2)}) copy-start(bf16[2048,512]{1,0:T(8,128)(2,1)} %wq_hbm.3) | copy-start | bytes 6291460
  20.7 6.1 %copy-start.9 = (bf16[2048,512]{1,0:T(8,128)(2,1)S(1)}, bf16[2048,512]{1,0:T(8,128)(2,1)}, u32[]{:S(2)}) copy-start(bf16[2048,512]{1,0:T(8,128)(2,1)} %wp_hbm.1) | copy-start | bytes 6291460
  26.8 12.9 %copy-start.10 = (bf16[2048,512]{1,0:T(8,128)(2,1)S(1)}, bf16[2048,512]{1,0:T(8,128)(2,1)}, u32[]{:S(2)}) copy-start(bf16[2048,512]{1,0:T(8,128)(2,1)} %wg_hbm.1) | copy-start | bytes 6291460
  26.9 12.9 %copy-start.11 = (bf16[2,256,256]{2,1,0:T(8,128)(2,1)S(1)}, bf16[2,256,256]{2,1,0:T(8,128)(2,1)}, u32[]{:S(2)}) copy-start(bf16[2,256,256]{2,1,0:T(8,128)(2,1)} %mix.1) | copy-start | bytes 786436
  26.9 12.9 %copy-start.13 = (f32[2,256]{1,0:T(2,128)S(1)}, f32[2,256]{1,0:T(2,128)}, u32[]{:S(2)}) copy-start(f32[2,256]{1,0:T(2,128)} %bias.1) | copy-start | bytes 6148
  26.9 12.9 %copy-start.14 = (f32[512]{0:T(512)S(1)}, f32[512]{0:T(512)}, u32[]{:S(2)}) copy-start(f32[512]{0:T(512)} %param.26) | copy-start | bytes 6148
  26.9 12.9 %copy-start.15 = (f32[512]{0:T(512)S(1)}, f32[512]{0:T(512)}, u32[]{:S(2)}) copy-start(f32[512]{0:T(512)} %param.27) | copy-start | bytes 6148
  31.7 7.3 %collective-permute-start.1 = (bf16[16,512]{1,0:T(8,128)(2,1)S(1)}, bf16[16,512]{1,0:T(8,128)(2,1)S(1)}, u32[]{:S(2)}, u32[]{:S(2)}) collective-permute-start(bf16[16,512]{1,0:T(8,128)(2,1)S(1)} %get-tuple-element.36), channel_id=1, source_target_pairs={{0,8},{8,16},{16,24},{24,32},{32,40},{40,48},{48,56},{56,64},{64,7... | collective-permute-start | bytes 49160 | tf_op jit(solution)/shard_map/ppermute | solution.py:430
  35.0 9.9 %collective-permute-start.2 = (bf16[512,128]{1,0:T(8,128)(2,1)S(1)}, bf16[512,128]{1,0:T(8,128)(2,1)S(1)}, u32[]{:S(2)}, u32[]{:S(2)}) collective-permute-start(bf16[512,128]{1,0:T(8,128)(2,1)S(1)} %get-tuple-element.38.own), channel_id=1, source_target_pairs={{0,8},{8,16},{16,24},{24,0},{1,9},{9,17},{17,25},{25,1},{2,10},{10... | collective-permute-start | bytes 393224 | tf_op jit(solution)/shard_map/ppermute | solution.py:422
  36.4 9.7 %collective-permute-start.3 = (bf16[512,128]{1,0:T(8,128)(2,1)S(1)}, bf16[512,128]{1,0:T(8,128)(2,1)S(1)}, u32[]{:S(2)}, u32[]{:S(2)}) collective-permute-start(bf16[512,128]{1,0:T(8,128)(2,1)S(1)} %get-tuple-element.38.own), channel_id=1, source_target_pairs={{0,16},{8,24},{16,0},{24,8},{1,17},{9,25},{17,1},{25,9},{2,18},{10... | collective-permute-start | bytes 393224 | tf_op jit(solution)/shard_map/ppermute | solution.py:422
  39.0 7.1 %collective-permute-start.4 = (bf16[512,128]{1,0:T(8,128)(2,1)S(1)}, bf16[512,128]{1,0:T(8,128)(2,1)S(1)}, u32[]{:S(2)}, u32[]{:S(2)}) collective-permute-start(bf16[512,128]{1,0:T(8,128)(2,1)S(1)} %get-tuple-element.38.own), channel_id=1, source_target_pairs={{0,24},{8,0},{16,8},{24,16},{1,25},{9,1},{17,9},{25,17},{2,26},{10... | collective-permute-start | bytes 393224 | tf_op jit(solution)/shard_map/ppermute | solution.py:422
  44.9 18.5 %collective-permute-start.8 = (bf16[512,512]{1,0:T(8,128)(2,1)S(1)}, bf16[512,512]{1,0:T(8,128)(2,1)S(1)}, u32[]{:S(2)}, u32[]{:S(2)}) collective-permute-start(bf16[512,512]{1,0:T(8,128)(2,1)S(1)} %get-tuple-element.43), channel_id=1, source_target_pairs={{0,1},{1,0},{2,3},{3,2},{4,5},{5,4},{6,7},{7,6},{8,9},{9,8},{10,11... | collective-permute-start | bytes 1572872 | tf_op jit(solution)/shard_map/ppermute | solution.py:366
  46.3 8.8 %collective-permute-start.5 = (bf16[512,128]{1,0:T(8,128)(2,1)S(1)}, bf16[512,128]{1,0:T(8,128)(2,1)S(1)}, u32[]{:S(2)}, u32[]{:S(2)}) collective-permute-start(bf16[512,128]{1,0:T(8,128)(2,1)S(1)} %get-tuple-element.40), channel_id=1, source_target_pairs={{0,32},{32,64},{64,96},{1,33},{33,65},{65,97},{2,34},{34,66},{66,9... | collective-permute-start | bytes 393224 | tf_op jit(solution)/shard_map/ppermute | solution.py:436
  49.9 9.0 %collective-permute-start.6 = (bf16[512,128]{1,0:T(8,128)(2,1)S(1)}, bf16[512,128]{1,0:T(8,128)(2,1)S(1)}, u32[]{:S(2)}, u32[]{:S(2)}) collective-permute-start(bf16[512,128]{1,0:T(8,128)(2,1)S(1)} %get-tuple-element.40), channel_id=1, source_target_pairs={{0,64},{32,96},{1,65},{33,97},{2,66},{34,98},{3,67},{35,99},{4,68}... | collective-permute-start | bytes 393224 | tf_op jit(solution)/shard_map/ppermute | solution.py:436
  55.1 5.7 %collective-permute-start.7 = (bf16[512,128]{1,0:T(8,128)(2,1)S(1)}, bf16[512,128]{1,0:T(8,128)(2,1)S(1)}, u32[]{:S(2)}, u32[]{:S(2)}) collective-permute-start(bf16[512,128]{1,0:T(8,128)(2,1)S(1)} %get-tuple-element.40), channel_id=1, source_target_pairs={{0,96},{1,97},{2,98},{3,99},{4,100},{5,101},{6,102},{7,103},{8,104... | collective-permute-start | bytes 393224 | tf_op jit(solution)/shard_map/ppermute | solution.py:436
  60.8 2.6 %copy-start.1 = (bf16[512,2048]{1,0:T(8,128)(2,1)S(1)}, bf16[512,2048]{1,0:T(8,128)(2,1)}, u32[]{:S(2)}) copy-start(bf16[512,2048]{1,0:T(8,128)(2,1)} %w_own_hbm.1) | copy-start | bytes 6291460
  61.6 6.7 %collective-permute-start.10 = (bf16[512,512]{1,0:T(8,128)(2,1)S(1)}, bf16[512,512]{1,0:T(8,128)(2,1)S(1)}, u32[]{:S(2)}, u32[]{:S(2)}) collective-permute-start(bf16[512,512]{1,0:T(8,128)(2,1)S(1)} %partner_retention.1), channel_id=1, source_target_pairs={{0,1},{1,0},{2,3},{3,2},{4,5},{5,4},{6,7},{7,6},{8,9},{9,8},{10,11... | collective-permute-start | bytes 1572872 | tf_op jit(solution)/shard_map/ppermute | solution.py:366
  63.4 2.7 %copy-start = (bf16[512,2048]{1,0:T(8,128)(2,1)S(1)}, bf16[512,2048]{1,0:T(8,128)(2,1)}, u32[]{:S(2)}) copy-start(bf16[512,2048]{1,0:T(8,128)(2,1)} %w_hbm.1) | copy-start | bytes 6291460
  (8 other events, 8.8 us)
